TPU v7x, 32 devices: a whole 2x2x4 slice. The times are simulated.
32 devices in a mesh: fs: 8 (over z, y), tp: 4 (over x, core).
Axes of the slice: x: 2, y: 2, z: 4, core: 2. Of those that a mesh axis runs over, the one named last changes fastest.
Arguments:
- cotangent: bfloat16 [5120, 1024], P('fs', 'tp'), may hold values from -6 to 6
- inputs: bfloat16 [5120, 1024], P('fs', 'tp'), may hold values from -6 to 6
- pre_act: bfloat16 [5120, 2112], P('fs'), may hold values from -6 to 6
- w_up: bfloat16 [2112, 1024], P('fs', 'tp'), may hold values from -0.1875 to 0.1875
- w_down: bfloat16 [2112, 1024], P('fs', 'tp'), may hold values from -0.125 to 0.125
Outputs:
- grad_input: bfloat16 [5120, 1024], P('fs', 'tp')
- grad_up: float32 [2112, 1024], P('fs', 'tp')
All inputs are finite; a program needn't handle non-finite values.
Results may differ from a plain program's by a relative error of at most 0.0049.
Values may be sent and summed in bfloat16 or wider, within the bound.
A program may use at most 64 MiB of HBM per device.

v0:
```python
import jax
import jax.numpy as jnp
from jax import lax
from jax.sharding import PartitionSpec as P


def times_rows(left, piece):
    return lax.dot_general(
        left, piece, (((1,), (1,)), ((), ())), preferred_element_type=jnp.float32
    )


def local(cotangent, inputs, pre_act, w_up, w_down):
    row_count = cotangent.shape[0]
    token_total = row_count * lax.axis_size("fs")
    full_cotangent = lax.all_gather(cotangent, "tp", axis=1, tiled=True)
    down_whole = lax.all_gather(w_down, "tp", axis=1, tiled=True)
    grad_hidden = times_rows(full_cotangent, lax.all_gather(down_whole, "fs", axis=0, tiled=True))
    grad_pre = (2.0 * grad_hidden * jnp.maximum(pre_act.astype(jnp.float32), 0.0)).astype(
        jnp.bfloat16
    )
    columns = grad_pre
    grad_input = jnp.dot(
        columns, lax.all_gather(w_up, "fs", axis=0, tiled=True), preferred_element_type=jnp.float32
    )
    columns = grad_pre
    grad_share = lax.psum_scatter(
        lax.dot_general(
            columns, inputs, (((0,), (0,)), ((), ())), preferred_element_type=jnp.float32
        ),
        "fs",
        scatter_dimension=0,
        tiled=True,
    )
    grad_up = grad_share / jnp.sqrt(jnp.float32(token_total))
    return (grad_input.astype(jnp.bfloat16), grad_up)


def solution(mesh):
    return jax.shard_map(
        local,
        mesh=mesh,
        in_specs=(P("fs", "tp"), P("fs", "tp"), P("fs", None), P("fs", "tp"), P("fs", "tp")),
        out_specs=(P("fs", "tp"), P("fs", "tp")),
        check_vma=False,
    )
```

profile of v0, /device:TPU:0, one launch (start us, length us, event | category | flops | bytes accessed | tf_op | source)
XLA Modules:
  0.0 227.8 jit_solution(900045571831877215)
XLA Ops:
  7.2 0.0 copy-start
  7.2 0.0 all-gather.4.cloned.1.call-start
  7.2 0.7 all-gather.4.cloned.1.call-update
  7.9 0.0 all-gather.6.cloned.1.call-start
  8.0 10.3 %all_gather.13 = bf16[264,1024]{1,0:T(8,128)(2,1)} all-gather(bf16[264,256]{1,0:T(8,128)(2,1)} %param.9), channel_id=1, replica_groups=mesh['fs'=8,'tp'=4] {'tp'}, dimensions={1}, use_global_device_ids=true | all-gather | bytes 675840 | tf_op jit(solution)/shard_map/all_gather | solution.py:17
  18.3 0.0 all-gather.6.cloned.1.call-update
  18.3 0.0 all-gather.8.cloned.1.call-start
  18.4 0.7 all-gather.8.cloned.1.call-update
  19.1 0.0 reduce-scatter.2.cloned.1.call-start
  19.1 11.5 %all-gather.4.cloned.1.call-done = bf16[640,1024]{1,0:T(8,128)(2,1)} async-done(((bf16[640,256]{1,0:T(8,128)(2,1)}), bf16[640,1024]{1,0:T(8,128)(2,1)}) %all-gather.4.cloned.1.call-update) | async-done | bytes 1310736 | tf_op jit(solution)/shard_map/all_gather | solution.py:16
  30.6 76.6 %all-gather.6.cloned.1.call-done = bf16[2112,1024]{1,0:T(8,128)(2,1)} async-done(((bf16[264,1024]{1,0:T(8,128)(2,1)}), bf16[2112,1024]{1,0:T(8,128)(2,1)}) %all-gather.6.cloned.1.call-update) | async-done | bytes 4325392 | tf_op jit(solution)/shard_map/all_gather | solution.py:18
  107.2 7.1 %fusion.1 = bf16[640,2112]{0,1:T(8,128)(2,1)S(1)} fusion(bf16[640,2112]{0,1:T(8,128)(2,1)} %param.7, bf16[640,1024]{1,0:T(8,128)(2,1)} %all-gather.4.cloned.1.call-done, bf16[2112,1024]{1,0:T(8,128)(2,1)} %all-gather.6.cloned.1.call-done), kind=kOutput, calls=%fused_computation.2 | convolution fusion | flops 2774999040 | bytes 11042816 | tf_op jit(solution)/shard_map/dot_general | solution.py:8
  114.4 0.0 copy-done
  114.4 2.4 %fusion.2 = f32[2112,256]{1,0:T(8,128)} fusion(bf16[640,2112]{0,1:T(8,128)(2,1)S(1)} %fusion.1, bf16[640,256]{1,0:T(8,128)(2,1)S(1)} %copy-done), kind=kOutput, calls=%fused_computation.5 | convolution fusion | flops 692060160 | bytes 5193728 | tf_op jit(solution)/shard_map/dot_general | solution.py:28
  116.7 0.0 reduce-scatter.2.cloned.1.call-update
  116.8 31.7 %all-gather.8.cloned.1.call-done = bf16[2112,256]{1,0:T(8,128)(2,1)} async-done(((bf16[264,256]{1,0:T(8,128)(2,1)}), bf16[2112,256]{1,0:T(8,128)(2,1)}) %all-gather.8.cloned.1.call-update) | async-done | bytes 1081360 | tf_op jit(solution)/shard_map/all_gather | solution.py:24
  148.5 2.9 %convolution_convert_fusion = bf16[640,256]{1,0:T(8,128)(2,1)} fusion(bf16[640,2112]{0,1:T(8,128)(2,1)S(1)} %fusion.1, bf16[2112,256]{1,0:T(8,128)(2,1)} %all-gather.8.cloned.1.call-done), kind=kOutput, calls=%fused_computation.3 | convolution fusion | flops 692224000 | bytes 4112384 | tf_op jit(solution)/shard_map/dot_general | solution.py:23
  151.4 68.2 %reduce-scatter.2.cloned.1.call-done = f32[264,256]{1,0:T(8,128)} async-done(((f32[2112,256]{1,0:T(8,128)}), f32[264,256]{1,0:T(8,128)}) %reduce-scatter.2.cloned.1.call-update) | async-done | bytes 270352 | tf_op jit(solution)/shard_map/reduce_scatter | solution.py:27
  219.6 1.7 broadcast_multiply_fusion
Async XLA Ops:
  7.2 107.2 %copy-start = (bf16[640,256]{1,0:T(8,128)(2,1)S(1)}, bf16[640,256]{1,0:T(8,128)(2,1)}, u32[]{:S(2)}) copy-start(bf16[640,256]{1,0:T(8,128)(2,1)} %param.6) | copy-start | bytes 983044
  7.2 23.4 %all-gather.4.cloned.1.call-start = ((), (), s32[]{:S(2)}) async-start(), calls=%async_computation.1 | async-start | bytes 1638400 | tf_op jit(solution)/shard_map/all_gather | solution.py:16
  7.9 99.3 %all-gather.6.cloned.1.call-start = ((), (), s32[]{:S(2)}) async-start(), calls=%async_computation.2 | async-start | bytes 4866048 | tf_op jit(solution)/shard_map/all_gather | solution.py:18
  18.3 130.1 %all-gather.8.cloned.1.call-start = ((), (), s32[]{:S(2)}) async-start(), calls=%async_computation.3 | async-start | bytes 1216512 | tf_op jit(solution)/shard_map/all_gather | solution.py:24
  19.1 200.5 %reduce-scatter.2.cloned.1.call-start = ((), (), s32[]{:S(2)}) async-start(), calls=%async_computation.4 | async-start | bytes 2433024 | tf_op jit(solution)/shard_map/reduce_scatter | solution.py:27
Sparse Core Ops, SparseCore 0:
  9.5 21.0 all-gather.3
  32.8 74.3 all-gather.5
  109.4 39.0 all-gather.7
  151.8 67.7 reduce-scatter.1
where the time goes:
time: 228 us
  waiting for transfers between devices  189 us (83%)
  between operations  13.8 us (6%)
  matrix products  12.4 us (5%)
  blocking collectives  10.3 us (5%)
    all_gather x1, waiting for transfers between devices, local(): lax.all_gather(down_whole, 'fs', axis=0, tiled=True)  76.6 us
    reduce_scatter x1, waiting for transfers between devices, local(): lax.psum_scatter(lax.dot_general(columns, inputs, (((0,), (0,)), ((), ())...  68.2 us
    all_gather x1, waiting for transfers between devices, local(): lax.all_gather(w_up, 'fs', axis=0, tiled=True)  31.7 us
    all_gather x1, waiting for transfers between devices, local(): full_cotangent = lax.all_gather(cotangent, 'tp', axis=1, tiled=True)  11.5 us
    all_gather x1, blocking collectives, local(): down_whole = lax.all_gather(w_down, 'tp', axis=1, tiled=True)  10.3 us
    dot_general x1, matrix products, times_rows(): lax.dot_general(left, piece, (((1,), (1,)), ((), ())), preferred_element_...  7.12 us
  transfers between devices with their start and end apart: 4, of which 4 were waited for; matrix products, arithmetic and copies ran while one was open for 5% of the time, Pallas kernels for 0%

commit v1 on v0

--- a/solution.py
+++ b/solution.py
@@ -15,7 +15,12 @@
     token_total = row_count * lax.axis_size("fs")
     full_cotangent = lax.all_gather(cotangent, "tp", axis=1, tiled=True)
     down_whole = lax.all_gather(w_down, "tp", axis=1, tiled=True)
-    grad_hidden = times_rows(full_cotangent, lax.all_gather(down_whole, "fs", axis=0, tiled=True))
+    grad_hidden = times_rows(
+        full_cotangent,
+        jnp.concatenate(
+            lax.all_to_all(jnp.stack([down_whole] * lax.axis_size("fs")), "fs", 0, 0), axis=0
+        ),
+    )
     grad_pre = (2.0 * grad_hidden * jnp.maximum(pre_act.astype(jnp.float32), 0.0)).astype(
         jnp.bfloat16
     )

time: 228 us -> 220 us (0.965)
  waiting for transfers between devices: 189 us -> 175 us
  starting transfers between devices: 0.16 us -> 5.95 us
  local copies, waits for them, and re-layouts: 0.01 us -> 2.61 us
    all_to_all x0 -> x1, waiting for transfers between devices: none -> 88 us  [local(): lax.all_to_all(jnp.stack([down_whole] * lax.axis_size('fs')), 'fs', 0, 0)]
    all_gather x1 -> x0, waiting for transfers between devices: 76.6 us -> none  [local(): lax.all_gather(down_whole, 'fs', axis=0, tiled=True)]
    all_gather x1, waiting for transfers between devices: 31.7 us -> 0.02 us  [local(): lax.all_gather(w_up, 'fs', axis=0, tiled=True)]
    all_gather x1, waiting for transfers between devices: 11.5 us -> 20.2 us  [local(): full_cotangent = lax.all_gather(cotangent, 'tp', axis=1, tiled=True)]
    all_to_all x0 -> x1, starting transfers between devices: none -> 5.83 us  [local(): lax.all_to_all(jnp.stack([down_whole] * lax.axis_size('fs')), 'fs', 0, 0)]
    reduce_scatter x1, waiting for transfers between devices: 68.2 us -> 65 us  [local(): lax.psum_scatter(lax.dot_general(columns, inputs, (((0,), (0,)), ((), ())...]
    another operation x0 -> x1, local copies, waits for them, and re-layouts: none -> 2.6 us  [local(): jnp.stack([down_whole] * lax.axis_size('fs'))]
  transfers between devices with their start and end apart: 4 -> 4, of which waited for: 4 -> 3; matrix products, arithmetic and copies ran while one was open for 5% -> 6% of each run, Pallas kernels for 0% -> 0%
where the time goes in v1:
time: 220 us
  waiting for transfers between devices  175 us (80%)
  between operations  13.8 us (6%)
  matrix products  12.4 us (6%)
  blocking collectives  9.08 us (4%)
  starting transfers between devices  5.95 us (3%)
  local copies, waits for them, and re-layouts  2.61 us (1%)
    all_to_all x1, waiting for transfers between devices, local(): lax.all_to_all(jnp.stack([down_whole] * lax.axis_size('fs')), 'fs', 0, 0)  88 us
    reduce_scatter x1, waiting for transfers between devices, local(): lax.psum_scatter(lax.dot_general(columns, inputs, (((0,), (0,)), ((), ())...  65 us
    all_gather x1, waiting for transfers between devices, local(): full_cotangent = lax.all_gather(cotangent, 'tp', axis=1, tiled=True)  20.2 us
    all_gather x1, blocking collectives, local(): down_whole = lax.all_gather(w_down, 'tp', axis=1, tiled=True)  9.08 us
    dot_general x1, matrix products, times_rows(): lax.dot_general(left, piece, (((1,), (1,)), ((), ())), preferred_element_...  7.12 us
    all_to_all x1, starting transfers between devices, local(): lax.all_to_all(jnp.stack([down_whole] * lax.axis_size('fs')), 'fs', 0, 0)  5.83 us
  transfers between devices with their start and end apart: 4, of which 3 were waited for; matrix products, arithmetic and copies ran while one was open for 6% of the time, Pallas kernels for 0%

profile of v1, /device:TPU:0, one launch (start us, length us, event | category | flops | bytes accessed | tf_op | source)
XLA Modules:
  0.0 220.0 jit_solution(6515564681647642604)
XLA Ops:
  7.2 0.0 copy-start
  7.2 9.1 %all_gather.10 = bf16[264,1024]{1,0:T(8,128)(2,1)S(1)} all-gather(bf16[264,256]{1,0:T(8,128)(2,1)} %param.9), channel_id=1, replica_groups=mesh['fs'=8,'tp'=4] {'tp'}, dimensions={1}, use_global_device_ids=true | all-gather | bytes 675840 | tf_op jit(solution)/shard_map/all_gather | solution.py:17
  16.3 2.6 %stack.2 = bf16[8,264,1024]{2,1,0:T(8,128)(2,1)} broadcast(bf16[264,1024]{1,0:T(8,128)(2,1)S(1)} %all_gather.10), dimensions={1,2} | broadcast | bytes 4866048 | tf_op jit(solution)/shard_map/stack | solution.py:21
  18.9 5.8 %all-to-all-start = ((bf16[8,264,1024]{2,1,0:T(8,128)(2,1)}), bf16[8,264,1024]{2,1,0:T(8,128)(2,1)}, u32[]{:S(2)}, u32[]{:S(2)}) async-start(bf16[8,264,1024]{2,1,0:T(8,128)(2,1)} %stack.2), calls=%async_computation | async-start | bytes 8650752 | tf_op jit(solution)/shard_map/all_to_all | solution.py:21
  24.7 0.0 all-gather.3.cloned.1.call-start
  24.7 0.7 all-gather.3.cloned.1.call-update
  25.4 0.0 all-gather.5.cloned.1.call-start
  25.5 0.7 all-gather.5.cloned.1.call-update
  26.2 0.0 reduce-scatter.2.cloned.1.call-start
  26.2 20.2 %all-gather.3.cloned.1.call-done = bf16[640,1024]{1,0:T(8,128)(2,1)} async-done(((bf16[640,256]{1,0:T(8,128)(2,1)}), bf16[640,1024]{1,0:T(8,128)(2,1)}) %all-gather.3.cloned.1.call-update) | async-done | bytes 1310736 | tf_op jit(solution)/shard_map/all_gather | solution.py:16
  46.4 88.0 %all-to-all-done = bf16[8,264,1024]{2,1,0:T(8,128)(2,1)} async-done(((bf16[8,264,1024]{2,1,0:T(8,128)(2,1)}), bf16[8,264,1024]{2,1,0:T(8,128)(2,1)}, u32[]{:S(2)}, u32[]{:S(2)}) %all-to-all-start) | async-done | bytes 4325408 | tf_op jit(solution)/shard_map/all_to_all | solution.py:21
  134.4 7.1 %fusion.1 = bf16[640,2112]{0,1:T(8,128)(2,1)S(1)} fusion(bf16[640,2112]{0,1:T(8,128)(2,1)} %param.7, bf16[640,1024]{1,0:T(8,128)(2,1)} %all-gather.3.cloned.1.call-done, bf16[2112,1024]{1,0:T(8,128)(2,1)} %bitcast), kind=kOutput, calls=%fused_computation.2 | convolution fusion | flops 2774999040 | bytes 11042816 | tf_op jit(solution)/shard_map/dot_general | solution.py:8
  141.5 0.0 copy-done
  141.5 2.4 %fusion.2 = f32[2112,256]{1,0:T(8,128)} fusion(bf16[640,2112]{0,1:T(8,128)(2,1)S(1)} %fusion.1, bf16[640,256]{1,0:T(8,128)(2,1)S(1)} %copy-done), kind=kOutput, calls=%fused_computation.5 | convolution fusion | flops 692060160 | bytes 5193728 | tf_op jit(solution)/shard_map/dot_general | solution.py:33
  143.9 0.0 reduce-scatter.2.cloned.1.call-update
  143.9 0.0 all-gather.5.cloned.1.call-done
  143.9 2.9 %convolution_convert_fusion = bf16[640,256]{1,0:T(8,128)(2,1)} fusion(bf16[640,2112]{0,1:T(8,128)(2,1)S(1)} %fusion.1, bf16[2112,256]{1,0:T(8,128)(2,1)} %all-gather.5.cloned.1.call-done), kind=kOutput, calls=%fused_computation.3 | convolution fusion | flops 692224000 | bytes 4112384 | tf_op jit(solution)/shard_map/dot_general | solution.py:28
  146.9 65.0 %reduce-scatter.2.cloned.1.call-done = f32[264,256]{1,0:T(8,128)} async-done(((f32[2112,256]{1,0:T(8,128)}), f32[264,256]{1,0:T(8,128)}) %reduce-scatter.2.cloned.1.call-update) | async-done | bytes 270352 | tf_op jit(solution)/shard_map/reduce_scatter | solution.py:32
  211.8 1.7 broadcast_multiply_fusion
Async XLA Ops:
  7.2 134.3 %copy-start = (bf16[640,256]{1,0:T(8,128)(2,1)S(1)}, bf16[640,256]{1,0:T(8,128)(2,1)}, u32[]{:S(2)}) copy-start(bf16[640,256]{1,0:T(8,128)(2,1)} %param.6) | copy-start | bytes 983044
  18.9 115.5 %all-to-all-start = ((bf16[8,264,1024]{2,1,0:T(8,128)(2,1)}), bf16[8,264,1024]{2,1,0:T(8,128)(2,1)}, u32[]{:S(2)}, u32[]{:S(2)}) async-start(bf16[8,264,1024]{2,1,0:T(8,128)(2,1)} %stack.2), calls=%async_computation | async-start | bytes 8650752 | tf_op jit(solution)/shard_map/all_to_all | solution.py:21
  24.7 21.7 %all-gather.3.cloned.1.call-start = ((), (), s32[]{:S(2)}) async-start(), calls=%async_computation.2 | async-start | bytes 1638400 | tf_op jit(solution)/shard_map/all_gather | solution.py:16
  25.4 118.5 %all-gather.5.cloned.1.call-start = ((), (), s32[]{:S(2)}) async-start(), calls=%async_computation.3 | async-start | bytes 1216512 | tf_op jit(solution)/shard_map/all_gather | solution.py:29
  26.2 185.6 %reduce-scatter.2.cloned.1.call-start = ((), (), s32[]{:S(2)}) async-start(), calls=%async_computation.4 | async-start | bytes 2433024 | tf_op jit(solution)/shard_map/reduce_scatter | solution.py:32
Sparse Core Ops, SparseCore 0:
  27.1 19.2 all-gather.2
  48.6 87.0 all-gather.4
  144.0 67.7 reduce-scatter.1
